TPU v7x, 256 devices: a 4x2x16 block of a 4x16x16 slice. The times are simulated.
256 devices in a mesh: grp: 2 (over y), sp: 16 (over z), tp: 8 (over x, core).
Axes of the slice: x: 4, y: 2, z: 16, core: 2. Of those that a mesh axis runs over, the one named last changes fastest.
The devices are a block of a 4x16x16 slice.
Arguments:
- tokens: bfloat16 [32, 4096, 4096], P(('grp', 'tp'), 'sp'), parts along dimension 0, may hold values from -8 to 8, as said below
- offsets: int32 [32], P(('grp', 'tp')), parts along dimension 0, may hold values from 0 to 4095
- in_gain: float32 [4096], replicated, may hold values from 0.1 to 1.9
- w_latent: bfloat16 [4096, 1024], P('sp'), may hold values from -0.09375 to 0.09375
- w_rope_key: bfloat16 [4096, 32], replicated, may hold values from -0.09375 to 0.09375
- kv_gain: float32 [1024], replicated, may hold values from 0.1 to 1.9
- w_up_key: bfloat16 [1024, 2048], P(None, 'tp'), may hold values from -0.1875 to 0.1875
- w_up_value: bfloat16 [1024, 2048], P(None, 'tp'), may hold values from -0.1875 to 0.1875
- q_nope: bfloat16 [32, 2048], P(('grp', 'sp'), 'tp'), parts along dimension 0, may hold values from -300 to 300, as said below
- q_rope: bfloat16 [32, 1024], P(('grp', 'sp'), 'tp'), parts along dimension 0, may hold values from -16 to 16
Outputs:
- keys: bfloat16 [32, 4096, 2048], P(('grp', 'sp'), None, 'tp'), parts along dimension 0
- values: bfloat16 [32, 4096, 2048], P(('grp', 'sp'), None, 'tp'), parts along dimension 0
- rope_keys: bfloat16 [32, 32, 4096], P(('grp', 'sp')), parts along dimension 0
- read: bfloat16 [32, 2048], P(('grp', 'sp'), 'tp'), parts along dimension 0
There are 2 independent parts, one for each index of `grp`. A program takes and returns all parts, laid end to end along the dimension named above; an argument that names none is the same for every part. Nothing has to cross between parts.
Inputs may be any that keep to these rules, and one draw needn't show every extreme that they name: `tokens`: entries of the layer's input. `q_nope`: entries of the first decoding token's queries.
All inputs are finite; a program needn't handle non-finite values.
Results may differ from a plain program's by a relative error of at most 0.02.
Values may be sent and summed in bfloat16 or wider, within the bound.
A program may use at most 128 MiB of HBM per device.

v0:
```python
import jax
import jax.numpy as jnp
from jax import lax
from jax.sharding import PartitionSpec as P

HEAD = 64
ROPE = 32
EPS = 1e-06


def joined_along(tiles, dim):
    shape = list(tiles.shape[1:])
    shape[dim] *= tiles.shape[0]
    return jnp.moveaxis(tiles, 0, dim).reshape(shape)


def copy_for_each(value, axis):
    peers = lax.axis_size(axis)
    return lax.all_to_all(
        jnp.broadcast_to(value[None], (peers, *value.shape)), axis, 0, 0, tiled=True
    )


def gather_directly(value, axis, dim):
    return joined_along(copy_for_each(value, axis), dim)


def rms_scale(values, gain):
    wide = values.astype(jnp.float32)
    return wide * lax.rsqrt(jnp.mean(wide * wide, axis=-1, keepdims=True) + EPS) * gain


def rotate(raw, position):
    inverse = 10000.0 ** (-jnp.arange(0, ROPE, 2).astype(jnp.float32) / ROPE)
    angle = position.astype(jnp.float32)[..., None] * inverse
    cosine, sine = (jnp.cos(angle), jnp.sin(angle))
    half = ROPE // 2
    first, second = (raw[..., :half], raw[..., half:])
    return jnp.concatenate(
        [first * cosine - second * sine, second * cosine + first * sine], axis=-1
    )


def local(
    tokens, offsets, in_gain, w_latent, w_rope_key, kv_gain, w_up_key, w_up_value, q_nope, q_rope
):
    prompts, rows, width = tokens.shape
    n_sp = lax.axis_size("sp")
    length = n_sp * rows
    block = lax.axis_index("sp")
    normed = rms_scale(tokens.reshape(prompts * rows, width), in_gain).astype(jnp.bfloat16)
    latent_raw = jnp.dot(
        normed,
        lax.all_gather(w_latent, "sp", axis=0, tiled=True),
        preferred_element_type=jnp.float32,
    )
    latent = rms_scale(latent_raw, kv_gain).astype(jnp.bfloat16)
    position = offsets[:, None] + block * rows + jnp.arange(rows, dtype=jnp.int32)[None, :]
    rope_raw = jnp.dot(normed, w_rope_key, preferred_element_type=jnp.float32).reshape(
        prompts, rows, ROPE
    )
    rotated = rotate(rope_raw, position).astype(jnp.bfloat16)
    head_cols = w_up_key.shape[1]
    paired = jnp.stack([w_up_key, w_up_value])
    both = jnp.einsum(
        "tk,skc->stc",
        latent,
        lax.all_gather(paired, "tp", axis=2, tiled=True),
        preferred_element_type=jnp.float32,
    ).astype(jnp.bfloat16)
    both = both.reshape(2, prompts, rows, both.shape[2])
    by_head = lax.all_to_all(both, "tp", split_axis=3, concat_axis=1, tiled=True)
    rope_every = gather_directly(rotated, "tp", 0)
    moved, rope_moved = (
        lax.all_to_all(by_head[:, :, None], "sp", split_axis=1, concat_axis=2, tiled=True),
        lax.all_to_all(rope_every[None, :, None], "sp", split_axis=1, concat_axis=2, tiled=True),
    )
    keys = moved[0].reshape(length, head_cols)
    values = moved[1].reshape(length, head_cols)
    rope_all = rope_moved.reshape(length, ROPE)
    rope_keys = rope_all.T
    heads_here = head_cols // HEAD
    query = q_nope.reshape(heads_here, HEAD)
    rotary_q = q_rope.reshape(heads_here, ROPE)
    keys_split = keys.reshape(length, heads_here, HEAD)
    scores = jnp.einsum("hd,jhd->hj", query, keys_split, preferred_element_type=jnp.float32)
    scores = scores + jnp.dot(rotary_q, rope_keys, preferred_element_type=jnp.float32)
    scores = scores / jnp.sqrt(jnp.float32(HEAD + ROPE))
    peak = jnp.max(scores, axis=-1, keepdims=True)
    expo = jnp.exp(scores - peak)
    weights = (expo / jnp.sum(expo, axis=-1, keepdims=True)).astype(jnp.bfloat16)
    read = jnp.einsum(
        "hj,jhd->hd",
        weights,
        values.reshape(length, heads_here, HEAD),
        preferred_element_type=jnp.float32,
    )
    read = read.astype(jnp.bfloat16).reshape(1, heads_here * HEAD)
    return (keys[None], values[None], rope_keys[None], read)


def solution(mesh):
    in_specs = (
        P(("grp", "tp"), "sp", None),
        P(("grp", "tp")),
        P(),
        P("sp", None),
        P(),
        P(),
        P(None, "tp"),
        P(None, "tp"),
        P(("grp", "sp"), "tp"),
        P(("grp", "sp"), "tp"),
    )
    out_specs = (
        P(("grp", "sp"), None, "tp"),
        P(("grp", "sp"), None, "tp"),
        P(("grp", "sp"), None, None),
        P(("grp", "sp"), "tp"),
    )
    return jax.shard_map(local, mesh=mesh, in_specs=in_specs, out_specs=out_specs, check_vma=False)
```

profile of v0, /device:TPU:33, one launch (start us, length us, event | category | flops | bytes accessed | tf_op | source)
XLA Modules:
  0.0 515.6 jit_solution(11231751343885072324)
XLA Ops:
  7.2 0.0 copy-start
  7.2 0.0 copy-start.6
  7.2 0.1 all-gather.5.cloned.1.call-start
  7.3 0.7 all-gather.5.cloned.1.call-update
  8.0 0.1 all-gather.3.cloned.1.call-start
  8.1 2.3 pad_maximum_fusion
  10.3 0.1 all-gather.3.cloned.1.call-update
  10.4 0.0 copy-start.3
  10.4 0.8 broadcast_add_fusion
  11.2 0.1 add_convert_fusion
  11.3 3.3 multiply_reduce_fusion
  14.6 0.0 copy-done
  14.6 0.0 copy-done.6
  14.6 0.0 copy-done.3
  14.7 1.4 fusion.4
  16.1 0.2 fusion.21
  16.4 0.8 broadcast_in_dim.7
  17.2 23.7 %all-to-all-start.2 = ((bf16[8,2,256,32]{2,1,3,0:T(2,128)(2,1)}), bf16[8,2,256,32]{2,1,3,0:T(2,128)(2,1)S(1)}, u32[]{:S(2)}, u32[]{:S(2)}) async-start(bf16[8,2,256,32]{2,1,3,0:T(2,128)(2,1)} %broadcast_in_dim.7), calls=%async_computation.2 | async-start | bytes 524288 | tf_op jit(solution)/shard_map/all_to_all | solution.py:19
  40.9 5.8 %fusion.1 = bf16[512,4096]{1,0:T(8,128)(2,1)} fusion(bf16[2,256,4096]{2,1,0:T(8,128)(2,1)} %param.10, f32[4096]{0:T(1024)S(1)} %copy-done.6, f32[512]{0:T(512)S(1)} %bitcast.76), kind=kLoop, calls=%fused_computation.2 | loop fusion | flops 8388608 | bytes 8407040 | tf_op jit(solution)/shard_map/convert_element_type | solution.py:51
  46.7 0.0 copy-start.8
  46.7 81.6 %all-gather.5.cloned.1.call-done = bf16[4096,1024]{1,0:T(8,128)(2,1)} async-done(((bf16[256,1024]{1,0:T(8,128)(2,1)}), bf16[4096,1024]{1,0:T(8,128)(2,1)}) %all-gather.5.cloned.1.call-update) | async-done | bytes 8388624 | tf_op jit(solution)/shard_map/all_gather | solution.py:54
  128.3 8.3 %multiply_reduce_fusion.1 = (f32[512]{0:T(512)S(1)}, f32[512,1024]{1,0:T(8,128)S(1)}) fusion(bf16[512,4096]{1,0:T(8,128)(2,1)} %fusion.1, bf16[4096,1024]{1,0:T(8,128)(2,1)} %all-gather.5.cloned.1.call-done), kind=kOutput, calls=%fused_computation.14 | convolution fusion | flops 4296015360 | bytes 14682112 | tf_op jit(solution)/shard_map/dot_general | solution.py:52
  136.6 52.3 %all-gather.3.cloned.1.call-done = bf16[2,1024,2048]{2,1,0:T(8,128)(2,1)} async-done(((bf16[2,1024,256]{2,1,0:T(8,128)(2,1)}), bf16[2,1024,2048]{2,1,0:T(8,128)(2,1)}) %all-gather.3.cloned.1.call-update) | async-done | bytes 8388624 | tf_op jit(solution)/shard_map/all_gather | solution.py:68
  188.9 0.0 copy-done.8
  188.9 9.6 %convolution_convert_fusion = bf16[2,2048,512]{1,2,0:T(8,128)(2,1)} fusion(bf16[2,1024,2048]{2,1,0:T(8,128)(2,1)} %all-gather.3.cloned.1.call-done, f32[512,1024]{1,0:T(8,128)S(1)} %get-tuple-element.11, f32[1024]{0:T(1024)S(1)} %copy-done.8, f32[512]{0:T(512)S(1)} %add_rsqrt_fusion), kind=kOutput, calls=%fused_computation.12 | convolution fusion | flops 4298637312 | bytes 14686208 | tf_op jit(solution)/shard_map/tk,skc->stc/dot_general | solution.py:65
  198.6 11.2 %copy.25 = bf16[2,2,256,2048]{2,1,0,3:T(2,128)(2,1)} copy(bf16[2,2,256,2048]{3,2,1,0:T(8,128)(2,1)} %bitcast.68) | data formatting | bytes 8388608 | tf_op jit(solution)/shard_map/reshape | solution.py:71
  209.8 0.0 all-to-all-done.2
  209.8 4.7 all-to-all-start
  214.4 0.7 copy.30
  215.2 48.1 %all-to-all-done = bf16[2,2,256,2048]{2,1,0,3:T(2,128)(2,1)} async-done(((bf16[2,2,256,2048]{2,1,0,3:T(2,128)(2,1)}), bf16[2,2,256,2048]{2,1,0,3:T(2,128)(2,1)}, u32[]{:S(2)}, u32[]{:S(2)}) %all-to-all-start) | async-done | bytes 4194336 | tf_op jit(solution)/shard_map/all_to_all | solution.py:72
  263.3 12.1 %all-to-all-start.3 = ((bf16[1,16,1,256,32]{3,4,2,0,1:T(8,128)(2,1)}), bf16[1,16,1,256,32]{3,4,2,0,1:T(8,128)(2,1)S(1)}, u32[]{:S(2)}, u32[]{:S(2)}) async-start(bf16[1,16,1,256,32]{3,4,2,0,1:T(8,128)(2,1)} %bitcast.13), calls=%async_computation.3 | async-start | bytes 524288 | tf_op jit(solution)/shard_map/all_to_all | solution.py:76
  275.4 4.9 copy.26
  280.4 7.7 %all-to-all-done.3 = bf16[1,16,1,256,32]{3,4,2,0,1:T(8,128)(2,1)S(1)} async-done(((bf16[1,16,1,256,32]{3,4,2,0,1:T(8,128)(2,1)}), bf16[1,16,1,256,32]{3,4,2,0,1:T(8,128)(2,1)S(1)}, u32[]{:S(2)}, u32[]{:S(2)}) %all-to-all-start.3) | async-done | bytes 262176 | tf_op jit(solution)/shard_map/all_to_all | solution.py:76
  288.1 0.0 copy-start.7
  288.1 0.0 copy-start.9
  288.1 11.6 %all-to-all-start.1 = ((bf16[2,16,1,256,256]{3,4,2,0,1:T(8,128)(2,1)}), bf16[2,16,1,256,256]{3,4,2,0,1:T(8,128)(2,1)}, u32[]{:S(2)}, u32[]{:S(2)}) async-start(bf16[2,16,1,256,256]{3,4,2,0,1:T(8,128)(2,1)} %bitcast.67), calls=%async_computation.1 | async-start | bytes 8388608 | tf_op jit(solution)/shard_map/all_to_all | solution.py:75
  299.7 0.0 copy-done.7
  299.7 0.1 reshape.142
  299.8 0.5 broadcast.98
  300.3 0.0 copy-done.9
  300.3 0.7 reduce.5
  301.0 0.1 reshape.132
  301.1 0.0 copy-start.5
  301.1 180.2 %all-to-all-done.1 = bf16[2,16,1,256,256]{3,4,2,0,1:T(8,128)(2,1)} async-done(((bf16[2,16,1,256,256]{3,4,2,0,1:T(8,128)(2,1)}), bf16[2,16,1,256,256]{3,4,2,0,1:T(8,128)(2,1)}, u32[]{:S(2)}, u32[]{:S(2)}) %all-to-all-start.1) | async-done | bytes 4194336 | tf_op jit(solution)/shard_map/all_to_all | solution.py:75
  481.3 2.6 fusion.26
  483.9 0.0 copy-start.2
  483.9 1.3 copy-done.2
  485.2 2.5 copy.34
  487.8 3.9 copy.40
  491.7 2.5 copy.33
  494.2 2.4 copy.39
  496.5 0.0 copy-start.4
  496.5 0.0 copy-start.1
  496.5 4.3 reshape_reshape_squeeze.6
  500.9 2.0 fusion.28
  502.8 0.0 copy-done.5
  502.8 0.3 fusion.27
  503.1 0.2 fusion.15
  503.3 0.1 fusion.24
  503.5 0.0 copy-done.4
  503.5 2.3 reshape_reshape_squeeze.7
  505.8 2.2 fusion.13
  508.0 0.7 reshape.133
  508.7 0.0 copy-done.1
  (9 shorter events, 0.1 us)
Async XLA Ops:
  7.2 7.4 %copy-start = (bf16[4096,32]{0,1:T(8,128)(2,1)S(1)}, bf16[4096,32]{0,1:T(8,128)(2,1)}, u32[]{:S(2)}) copy-start(bf16[4096,32]{0,1:T(8,128)(2,1)} %param.14) | copy-start | bytes 786436
  7.2 7.4 %copy-start.6 = (f32[4096]{0:T(1024)S(1)}, f32[4096]{0:T(1024)}, u32[]{:S(2)}) copy-start(f32[4096]{0:T(1024)} %param.12) | copy-start | bytes 49156
  7.2 121.1 %all-gather.5.cloned.1.call-start = ((), (), s32[]{:S(2)}) async-start(), calls=%async_computation.5 | async-start | bytes 8912896 | tf_op jit(solution)/shard_map/all_gather | solution.py:54
  8.0 180.9 %all-gather.3.cloned.1.call-start = ((), (), s32[]{:S(2)}) async-start(), calls=%async_computation.4 | async-start | bytes 9437184 | tf_op jit(solution)/shard_map/all_gather | solution.py:68
  10.4 4.2 copy-start.3
  17.2 192.6 %all-to-all-start.2 = ((bf16[8,2,256,32]{2,1,3,0:T(2,128)(2,1)}), bf16[8,2,256,32]{2,1,3,0:T(2,128)(2,1)S(1)}, u32[]{:S(2)}, u32[]{:S(2)}) async-start(bf16[8,2,256,32]{2,1,3,0:T(2,128)(2,1)} %broadcast_in_dim.7), calls=%async_computation.2 | async-start | bytes 524288 | tf_op jit(solution)/shard_map/all_to_all | solution.py:19
  46.7 142.2 %copy-start.8 = (f32[1024]{0:T(1024)S(1)}, f32[1024]{0:T(1024)}, u32[]{:S(2)}) copy-start(f32[1024]{0:T(1024)} %param.15) | copy-start | bytes 12292
  209.8 53.6 %all-to-all-start = ((bf16[2,2,256,2048]{2,1,0,3:T(2,128)(2,1)}), bf16[2,2,256,2048]{2,1,0,3:T(2,128)(2,1)}, u32[]{:S(2)}, u32[]{:S(2)}) async-start(bf16[2,2,256,2048]{2,1,0,3:T(2,128)(2,1)} %copy.25), calls=%async_computation | async-start | bytes 8388608 | tf_op jit(solution)/shard_map/all_to_all | solution.py:72
  263.3 24.8 %all-to-all-start.3 = ((bf16[1,16,1,256,32]{3,4,2,0,1:T(8,128)(2,1)}), bf16[1,16,1,256,32]{3,4,2,0,1:T(8,128)(2,1)S(1)}, u32[]{:S(2)}, u32[]{:S(2)}) async-start(bf16[1,16,1,256,32]{3,4,2,0,1:T(8,128)(2,1)} %bitcast.13), calls=%async_computation.3 | async-start | bytes 524288 | tf_op jit(solution)/shard_map/all_to_all | solution.py:76
  288.1 11.6 %copy-start.7 = (bf16[1,256]{1,0:T(2,128)(2,1)S(1)}, bf16[1,256]{1,0:T(2,128)(2,1)}, u32[]{:S(2)}) copy-start(bf16[1,256]{1,0:T(2,128)(2,1)} %param.18) | copy-start | bytes 1540
  288.1 12.2 %copy-start.9 = (bf16[1,128]{1,0:T(2,128)(2,1)S(1)}, bf16[1,128]{1,0:T(2,128)(2,1)}, u32[]{:S(2)}) copy-start(bf16[1,128]{1,0:T(2,128)(2,1)} %param.19) | copy-start | bytes 772
  288.1 193.2 %all-to-all-start.1 = ((bf16[2,16,1,256,256]{3,4,2,0,1:T(8,128)(2,1)}), bf16[2,16,1,256,256]{3,4,2,0,1:T(8,128)(2,1)}, u32[]{:S(2)}, u32[]{:S(2)}) async-start(bf16[2,16,1,256,256]{3,4,2,0,1:T(8,128)(2,1)} %bitcast.67), calls=%async_computation.1 | async-start | bytes 8388608 | tf_op jit(solution)/shard_map/all_to_all | solution.py:75
  301.1 201.8 %copy-start.5 = (bf16[4,8,16,256]{3,1,2,0:T(8,128)(2,1)}, bf16[4,8,16,256]{3,1,2,0:T(8,128)(2,1)S(1)}, u32[]{:S(2)}) copy-start(bf16[4,8,16,256]{3,1,2,0:T(8,128)(2,1)S(1)} %copy.44) | copy-start | bytes 786436
  483.9 1.3 copy-start.2
  496.5 6.9 %copy-start.4 = (bf16[1,16,1,256,256]{3,1,4,2,0:T(8,128)(2,1)S(1)}, bf16[1,16,1,256,256]{3,1,4,2,0:T(8,128)(2,1)}, u32[]{:S(2)}) copy-start(bf16[1,16,1,256,256]{3,1,4,2,0:T(8,128)(2,1)} %copy.34) | copy-start | bytes 6291460
  496.5 12.2 %copy-start.1 = (bf16[4096,32]{0,1:T(8,128)(2,1)S(1)}, bf16[4096,32]{0,1:T(8,128)(2,1)}, u32[]{:S(2)}) copy-start(bf16[4096,32]{0,1:T(8,128)(2,1)} %param.14) | copy-start | bytes 786436
Sparse Core Ops, SparseCore 0:
  9.8 118.4 all-gather.4
  130.7 58.1 all-gather.2
where the time goes:
time: 517 us; the launch traced here: 516 us
  waiting for transfers between devices  371 us (72%)
  starting transfers between devices  52.2 us (10%)
  local copies, waits for them, and re-layouts  41 us (8%)
  matrix products  23.8 us (5%)
  between operations  14.2 us (3%)
  other arithmetic  13.5 us (3%)
    all_to_all x1, waiting for transfers between devices, local(): lax.all_to_all(by_head[:, :, None], 'sp', split_axis=1, concat_axis=2, ti...  180 us
    all_gather x1, waiting for transfers between devices, local(): lax.all_gather(w_latent, 'sp', axis=0, tiled=True)  81.6 us
    all_gather x1, waiting for transfers between devices, local(): lax.all_gather(paired, 'tp', axis=2, tiled=True)  52.3 us
    all_to_all x1, waiting for transfers between devices, local(): lax.all_to_all(both, 'tp', split_axis=3, concat_axis=1, tiled=True)  48.1 us
    all_to_all x1, starting transfers between devices, copy_for_each(): lax.all_to_all(jnp.broadcast_to(value[None], (peers, *value.shape)), axis...  23.7 us
    all_to_all x1, starting transfers between devices, local(): lax.all_to_all(rope_every[None, :, None], 'sp', split_axis=1, concat_axis...  12.1 us
    all_to_all x1, starting transfers between devices, local(): lax.all_to_all(by_head[:, :, None], 'sp', split_axis=1, concat_axis=2, ti...  11.6 us
    reshape x1, local copies, waits for them, and re-layouts, local(): both = both.reshape(2, prompts, rows, both.shape[2])  11.2 us
  transfers between devices with their start and end apart: 6, of which 5 were waited for; matrix products, arithmetic and copies ran while one was open for 10% of the time, Pallas kernels for 0%

commit v1 on v0

--- a/solution.py
+++ b/solution.py
@@ -65,7 +65,9 @@
     both = jnp.einsum(
         "tk,skc->stc",
         latent,
-        lax.all_gather(paired, "tp", axis=2, tiled=True),
+        jnp.concatenate(
+            lax.all_to_all(jnp.stack([paired] * lax.axis_size("tp")), "tp", 0, 0), axis=2
+        ),
         preferred_element_type=jnp.float32,
     ).astype(jnp.bfloat16)
     both = both.reshape(2, prompts, rows, both.shape[2])

time: 517 us -> 471 us (0.911)
  waiting for transfers between devices: 371 us -> 320 us
  local copies, waits for them, and re-layouts: 41 us -> 52.8 us
    all_to_all x0 -> x1, waiting for transfers between devices: none -> 82.8 us  [local(): lax.all_to_all(jnp.stack([paired] * lax.axis_size('tp')), 'tp', 0, 0)]
    all_gather x1, waiting for transfers between devices: 81.6 us -> 0.01 us  [local(): lax.all_gather(w_latent, 'sp', axis=0, tiled=True)]
    all_gather x1 -> x0, waiting for transfers between devices: 52.3 us -> none  [local(): lax.all_gather(paired, 'tp', axis=2, tiled=True)]
    all_to_all x0 -> x1, starting transfers between devices: none -> 25.3 us  [local(): lax.all_to_all(jnp.stack([paired] * lax.axis_size('tp')), 'tp', 0, 0)]
    all_to_all x1, starting transfers between devices: 23.7 us -> 4.28 us  [copy_for_each(): lax.all_to_all(jnp.broadcast_to(value[None], (peers, *value.shape)), axis...]
    reshape x0 -> x1, local copies, waits for them, and re-layouts: none -> 7.78 us  [local(): jnp.concatenate(lax.all_to_all(jnp.stack([paired] * lax.axis_size('tp')),...]
    all_to_all x1, starting transfers between devices: 12.1 us -> 4.71 us  [local(): lax.all_to_all(rope_every[None, :, None], 'sp', split_axis=1, concat_axis...]
  transfers between devices with their start and end apart: 6 -> 6, of which waited for: 5 -> 4; matrix products, arithmetic and copies ran while one was open for 10% -> 12% of each run, Pallas kernels for 0% -> 0%
where the time goes in v1:
time: 471 us; the launch traced here: 470 us
  waiting for transfers between devices  320 us (68%)
  local copies, waits for them, and re-layouts  52.8 us (11%)
  starting transfers between devices  50.8 us (11%)
  matrix products  22.9 us (5%)
  between operations  14.3 us (3%)
  other arithmetic  9.49 us (2%)
    all_to_all x1, waiting for transfers between devices, local(): lax.all_to_all(by_head[:, :, None], 'sp', split_axis=1, concat_axis=2, ti...  180 us
    all_to_all x1, waiting for transfers between devices, local(): lax.all_to_all(jnp.stack([paired] * lax.axis_size('tp')), 'tp', 0, 0)  82.8 us
    all_to_all x1, waiting for transfers between devices, local(): lax.all_to_all(both, 'tp', split_axis=3, concat_axis=1, tiled=True)  48 us
    all_to_all x1, starting transfers between devices, local(): lax.all_to_all(jnp.stack([paired] * lax.axis_size('tp')), 'tp', 0, 0)  25.3 us
    all_to_all x1, starting transfers between devices, local(): lax.all_to_all(by_head[:, :, None], 'sp', split_axis=1, concat_axis=2, ti...  11.6 us
    reshape x1, local copies, waits for them, and re-layouts, local(): both = both.reshape(2, prompts, rows, both.shape[2])  11.2 us
  transfers between devices with their start and end apart: 6, of which 4 were waited for; matrix products, arithmetic and copies ran while one was open for 12% of the time, Pallas kernels for 0%

profile of v1, /device:TPU:33, one launch (start us, length us, event | category | flops | bytes accessed | tf_op | source)
XLA Modules:
  0.0 469.8 jit_solution(6129602630136782383)
XLA Ops:
  7.2 0.0 copy-start
  7.2 0.1 all-gather.2.cloned.1.call-start
  7.3 0.7 all-gather.2.cloned.1.call-update
  8.0 1.3 pad_maximum_fusion
  9.3 4.0 stack.11
  13.3 25.3 %all-to-all-start = ((bf16[8,2,1024,256]{3,2,1,0:T(8,128)(2,1)}), bf16[8,2,1024,256]{3,2,1,0:T(8,128)(2,1)}, u32[]{:S(2)}, u32[]{:S(2)}) async-start(bf16[8,2,1024,256]{3,2,1,0:T(8,128)(2,1)} %stack.11), calls=%async_computation | async-start | bytes 16777216 | tf_op jit(solution)/shard_map/all_to_all | solution.py:69
  38.6 0.0 copy-start.10
  38.6 0.0 copy-start.7
  38.7 3.3 multiply_reduce_fusion
  41.9 0.0 copy-start.3
  42.0 0.0 copy-done.10
  42.0 0.1 add_convert_fusion
  42.1 0.0 copy-done
  42.1 0.0 copy-done.7
  42.1 3.8 fusion.4
  45.8 0.2 fusion.21
  46.1 0.0 copy-done.3
  46.1 3.6 fusion.1
  49.7 82.8 %all-to-all-done = bf16[8,2,1024,256]{3,2,1,0:T(8,128)(2,1)} async-done(((bf16[8,2,1024,256]{3,2,1,0:T(8,128)(2,1)}), bf16[8,2,1024,256]{3,2,1,0:T(8,128)(2,1)}, u32[]{:S(2)}, u32[]{:S(2)}) %all-to-all-start) | async-done | bytes 8388640 | tf_op jit(solution)/shard_map/all_to_all | solution.py:69
  132.5 0.8 broadcast_in_dim.7
  133.3 4.3 all-to-all-start.3
  137.6 7.8 %copy.45 = bf16[8,2,128,8,256]{4,3,0,2,1:T(8,128)(2,1)} copy(bf16[8,2,128,8,256]{4,3,2,1,0:T(8,128)(2,1)} %bitcast.26) | data formatting | bytes 16777216 | tf_op jit(solution)/shard_map/reshape | solution.py:68
  145.4 0.0 copy-start.9
  145.4 0.0 all-gather.2.cloned.1.call-done
  145.4 0.0 copy-start.4
  145.4 8.4 %multiply_reduce_fusion.1 = (f32[512]{0:T(512)S(1)}, f32[512,1024]{1,0:T(8,128)S(1)}) fusion(bf16[512,4096]{1,0:T(8,128)(2,1)} %fusion.1, bf16[4096,1024]{1,0:T(8,128)(2,1)} %all-gather.2.cloned.1.call-done), kind=kOutput, calls=%fused_computation.14 | convolution fusion | flops 4296015360 | bytes 14682112 | tf_op jit(solution)/shard_map/dot_general | solution.py:52
  153.8 0.0 copy-done.9
  153.8 0.0 copy-done.4
  153.9 6.2 %convolution_convert_fusion = bf16[2,2048,512]{1,2,0:T(8,128)(2,1)} fusion(bf16[2,1024,2048]{2,1,0:T(8,128)(2,1)S(1)} %bitcast.71, f32[512,1024]{1,0:T(8,128)S(1)} %get-tuple-element.11, f32[1024]{0:T(1024)S(1)} %copy-done.9, f32[512]{0:T(512)S(1)} %add_rsqrt_fusion), kind=kOutput, calls=%fused_computation.12 | convolution fusion | flops 4298637312 | bytes 14686208 | tf_op jit(solution)/shard_map/tk,skc->stc/dot_general | solution.py:65
  160.1 11.2 %copy.27 = bf16[2,2,256,2048]{2,1,0,3:T(2,128)(2,1)} copy(bf16[2,2,256,2048]{3,2,1,0:T(8,128)(2,1)} %bitcast.72) | data formatting | bytes 8388608 | tf_op jit(solution)/shard_map/reshape | solution.py:73
  171.2 0.0 all-to-all-done.3
  171.2 4.9 %all-to-all-start.1 = ((bf16[2,2,256,2048]{2,1,0,3:T(2,128)(2,1)}), bf16[2,2,256,2048]{2,1,0,3:T(2,128)(2,1)}, u32[]{:S(2)}, u32[]{:S(2)}) async-start(bf16[2,2,256,2048]{2,1,0,3:T(2,128)(2,1)} %copy.27), calls=%async_computation.1 | async-start | bytes 8388608 | tf_op jit(solution)/shard_map/all_to_all | solution.py:74
  176.1 0.7 copy.32
  176.9 48.0 %all-to-all-done.1 = bf16[2,2,256,2048]{2,1,0,3:T(2,128)(2,1)} async-done(((bf16[2,2,256,2048]{2,1,0,3:T(2,128)(2,1)}), bf16[2,2,256,2048]{2,1,0,3:T(2,128)(2,1)}, u32[]{:S(2)}, u32[]{:S(2)}) %all-to-all-start.1) | async-done | bytes 4194336 | tf_op jit(solution)/shard_map/all_to_all | solution.py:74
  224.9 4.7 %all-to-all-start.4 = ((bf16[1,16,1,256,32]{3,4,2,0,1:T(8,128)(2,1)}), bf16[1,16,1,256,32]{3,4,2,0,1:T(8,128)(2,1)S(1)}, u32[]{:S(2)}, u32[]{:S(2)}) async-start(bf16[1,16,1,256,32]{3,4,2,0,1:T(8,128)(2,1)} %bitcast.14), calls=%async_computation.4 | async-start | bytes 524288 | tf_op jit(solution)/shard_map/all_to_all | solution.py:78
  229.6 4.9 %copy.28 = bf16[2,8,2,256,256]{3,4,0,2,1:T(8,128)(2,1)} copy(bf16[2,8,2,256,256]{3,2,0,4,1:T(2,128)(2,1)} %bitcast.8) | data formatting | bytes 8388608 | tf_op jit(solution)/shard_map/all_to_all | solution.py:74
  234.6 7.8 %all-to-all-done.4 = bf16[1,16,1,256,32]{3,4,2,0,1:T(8,128)(2,1)S(1)} async-done(((bf16[1,16,1,256,32]{3,4,2,0,1:T(8,128)(2,1)}), bf16[1,16,1,256,32]{3,4,2,0,1:T(8,128)(2,1)S(1)}, u32[]{:S(2)}, u32[]{:S(2)}) %all-to-all-start.4) | async-done | bytes 262176 | tf_op jit(solution)/shard_map/all_to_all | solution.py:78
  242.3 11.6 %all-to-all-start.2 = ((bf16[2,16,1,256,256]{3,4,2,0,1:T(8,128)(2,1)}), bf16[2,16,1,256,256]{3,4,2,0,1:T(8,128)(2,1)}, u32[]{:S(2)}, u32[]{:S(2)}) async-start(bf16[2,16,1,256,256]{3,4,2,0,1:T(8,128)(2,1)} %bitcast.70), calls=%async_computation.2 | async-start | bytes 8388608 | tf_op jit(solution)/shard_map/all_to_all | solution.py:77
  253.9 0.0 copy-done.8
  253.9 0.1 reshape.152
  254.0 0.5 broadcast.100
  254.5 0.0 copy-done.11
  254.5 0.7 reduce.5
  255.2 0.1 reshape.142
  255.3 0.0 copy-start.6
  255.3 180.2 %all-to-all-done.2 = bf16[2,16,1,256,256]{3,4,2,0,1:T(8,128)(2,1)} async-done(((bf16[2,16,1,256,256]{3,4,2,0,1:T(8,128)(2,1)}), bf16[2,16,1,256,256]{3,4,2,0,1:T(8,128)(2,1)}, u32[]{:S(2)}, u32[]{:S(2)}) %all-to-all-start.2) | async-done | bytes 4194336 | tf_op jit(solution)/shard_map/all_to_all | solution.py:77
  435.6 2.6 fusion.26
  438.1 0.0 copy-start.2
  438.2 1.3 copy-done.2
  439.5 2.5 copy.35
  442.0 3.9 copy.41
  445.9 2.5 copy.36
  448.4 2.4 copy.42
  450.8 4.3 reshape_reshape_squeeze.6
  455.1 2.0 fusion.28
  457.1 0.0 copy-done.6
  457.1 0.3 fusion.27
  457.3 0.2 fusion.15
  457.6 0.1 fusion.24
  457.7 0.0 copy-done.5
  457.7 2.4 reshape_reshape_squeeze.7
  460.1 2.2 fusion.13
  462.3 0.7 reshape.143
  463.0 0.0 copy-done.1
  (14 shorter events, 0.1 us)
Async XLA Ops:
  7.2 34.9 %copy-start = (bf16[4096,32]{0,1:T(8,128)(2,1)S(1)}, bf16[4096,32]{0,1:T(8,128)(2,1)}, u32[]{:S(2)}) copy-start(bf16[4096,32]{0,1:T(8,128)(2,1)} %param.14) | copy-start | bytes 786436
  7.2 138.2 %all-gather.2.cloned.1.call-start = ((), (), s32[]{:S(2)}) async-start(), calls=%async_computation.5 | async-start | bytes 8912896 | tf_op jit(solution)/shard_map/all_gather | solution.py:54
  13.3 119.1 %all-to-all-start = ((bf16[8,2,1024,256]{3,2,1,0:T(8,128)(2,1)}), bf16[8,2,1024,256]{3,2,1,0:T(8,128)(2,1)}, u32[]{:S(2)}, u32[]{:S(2)}) async-start(bf16[8,2,1024,256]{3,2,1,0:T(8,128)(2,1)} %stack.11), calls=%async_computation | async-start | bytes 16777216 | tf_op jit(solution)/shard_map/all_to_all | solution.py:69
  38.6 3.3 copy-start.10
  38.6 3.4 copy-start.7
  41.9 4.2 copy-start.3
  133.3 37.9 %all-to-all-start.3 = ((bf16[8,2,256,32]{2,1,3,0:T(2,128)(2,1)}), bf16[8,2,256,32]{2,1,3,0:T(2,128)(2,1)S(1)}, u32[]{:S(2)}, u32[]{:S(2)}) async-start(bf16[8,2,256,32]{2,1,3,0:T(2,128)(2,1)} %broadcast_in_dim.7), calls=%async_computation.3 | async-start | bytes 524288 | tf_op jit(solution)/shard_map/all_to_all | solution.py:19
  145.4 8.5 %copy-start.9 = (f32[1024]{0:T(1024)S(1)}, f32[1024]{0:T(1024)}, u32[]{:S(2)}) copy-start(f32[1024]{0:T(1024)} %param.15) | copy-start | bytes 12292
  145.4 8.5 %copy-start.4 = (bf16[8,2,128,8,256]{4,3,0,2,1:T(8,128)(2,1)S(1)}, bf16[8,2,128,8,256]{4,3,0,2,1:T(8,128)(2,1)}, u32[]{:S(2)}) copy-start(bf16[8,2,128,8,256]{4,3,0,2,1:T(8,128)(2,1)} %copy.45) | copy-start | bytes 25165828
  171.2 53.7 %all-to-all-start.1 = ((bf16[2,2,256,2048]{2,1,0,3:T(2,128)(2,1)}), bf16[2,2,256,2048]{2,1,0,3:T(2,128)(2,1)}, u32[]{:S(2)}, u32[]{:S(2)}) async-start(bf16[2,2,256,2048]{2,1,0,3:T(2,128)(2,1)} %copy.27), calls=%async_computation.1 | async-start | bytes 8388608 | tf_op jit(solution)/shard_map/all_to_all | solution.py:74
  224.9 17.4 %all-to-all-start.4 = ((bf16[1,16,1,256,32]{3,4,2,0,1:T(8,128)(2,1)}), bf16[1,16,1,256,32]{3,4,2,0,1:T(8,128)(2,1)S(1)}, u32[]{:S(2)}, u32[]{:S(2)}) async-start(bf16[1,16,1,256,32]{3,4,2,0,1:T(8,128)(2,1)} %bitcast.14), calls=%async_computation.4 | async-start | bytes 524288 | tf_op jit(solution)/shard_map/all_to_all | solution.py:78
  242.3 11.6 %copy-start.8 = (bf16[1,256]{1,0:T(2,128)(2,1)S(1)}, bf16[1,256]{1,0:T(2,128)(2,1)}, u32[]{:S(2)}) copy-start(bf16[1,256]{1,0:T(2,128)(2,1)} %param.18) | copy-start | bytes 1540
  242.3 12.2 %copy-start.11 = (bf16[1,128]{1,0:T(2,128)(2,1)S(1)}, bf16[1,128]{1,0:T(2,128)(2,1)}, u32[]{:S(2)}) copy-start(bf16[1,128]{1,0:T(2,128)(2,1)} %param.19) | copy-start | bytes 772
  242.3 193.2 %all-to-all-start.2 = ((bf16[2,16,1,256,256]{3,4,2,0,1:T(8,128)(2,1)}), bf16[2,16,1,256,256]{3,4,2,0,1:T(8,128)(2,1)}, u32[]{:S(2)}, u32[]{:S(2)}) async-start(bf16[2,16,1,256,256]{3,4,2,0,1:T(8,128)(2,1)} %bitcast.70), calls=%async_computation.2 | async-start | bytes 8388608 | tf_op jit(solution)/shard_map/all_to_all | solution.py:77
  255.3 201.8 %copy-start.6 = (bf16[4,8,16,256]{3,1,2,0:T(8,128)(2,1)}, bf16[4,8,16,256]{3,1,2,0:T(8,128)(2,1)S(1)}, u32[]{:S(2)}) copy-start(bf16[4,8,16,256]{3,1,2,0:T(8,128)(2,1)S(1)} %copy.47) | copy-start | bytes 786436
  438.1 1.3 copy-start.2
  450.7 6.9 %copy-start.5 = (bf16[1,16,1,256,256]{3,1,4,2,0:T(8,128)(2,1)S(1)}, bf16[1,16,1,256,256]{3,1,4,2,0:T(8,128)(2,1)}, u32[]{:S(2)}) copy-start(bf16[1,16,1,256,256]{3,1,4,2,0:T(8,128)(2,1)} %copy.36) | copy-start | bytes 6291460
  450.7 12.2 %copy-start.1 = (bf16[4096,32]{0,1:T(8,128)(2,1)S(1)}, bf16[4096,32]{0,1:T(8,128)(2,1)}, u32[]{:S(2)}) copy-start(bf16[4096,32]{0,1:T(8,128)(2,1)} %param.14) | copy-start | bytes 786436
Sparse Core Ops, SparseCore 0:
  9.8 118.4 all-gather.1
